TPU v7x, 32 devices: a whole 2x2x4 slice. The times are simulated.
32 devices in a mesh: sp: 8 (over z, x), tp: 4 (over y, core).
Axes of the slice: x: 2, y: 2, z: 4, core: 2. Of those that a mesh axis runs over, the one named last changes fastest.
Arguments:
- queries: bfloat16 [8192, 1536], P('sp', 'tp'), may hold values from -200 to 200
- key_heads: bfloat16 [8192, 512], P('sp', 'tp'), may hold values from -6 to 6
- projected_value_heads: bfloat16 [8192, 512], P('sp', 'tp'), may hold values from -5 to 5
- sink_logit_table: float32 [24], P('tp'), may hold values from 0 to 4
- out_weight: bfloat16 [1536, 3072], P('tp'), may hold values from -1.5 to 1.5
- residual: bfloat16 [8192, 3072], P('sp', 'tp'), may hold values from -16 to 16
- norm_gain: bfloat16 [3072], P('tp'), may hold values from 0.099609375 to 1.8984375
- up_weight: bfloat16 [3072, 12288], P('sp', 'tp'), may hold values from -0.109375 to 0.109375
- down_weight: bfloat16 [12288, 3072], P('tp', 'sp'), may hold values from -0.0546875 to 0.0546875
Outputs:
- result: bfloat16 [8192, 3072], P('sp', 'tp')
All inputs are finite; a program needn't handle non-finite values.
Results may differ from a plain program's by a relative error of at most 0.015.
Values may be sent and summed in bfloat16 or wider, within the bound.
No kernel may reach another device: no remote copies, remote signals or barrier semaphores. Data moves between devices by JAX's collectives and lax.ppermute only.
A program may use at most 128 MiB of HBM per device.

v0:
```python
import jax
import jax.numpy as jnp
from jax import lax
from jax.sharding import PartitionSpec as P

D = 3072
HEAD_SIZE = 64
WINDOW_SPAN = 128
epsilon = 1e-06


def shifted(block, axis, distance):
    devices = range(lax.axis_size(axis))
    route = [(i - distance, i) for i in devices if i - distance in devices]
    return lax.ppermute(block, axis, route)


def attend(queries, key_heads, projected_value_heads, sink_logit_table, previous, offset):
    row_count = queries.shape[0]
    kv_cols = key_heads.shape[1]
    kv_local = kv_cols // HEAD_SIZE
    group_count = queries.shape[1] // kv_cols
    block_count = row_count // WINDOW_SPAN
    extended_keys = jnp.concatenate([previous[:, :kv_cols], key_heads], axis=0)
    extended_values = jnp.concatenate([previous[:, kv_cols:], projected_value_heads], axis=0)

    def banded(source_rows):
        shaped = source_rows.reshape(block_count + 1, WINDOW_SPAN, kv_local, HEAD_SIZE)
        return jnp.concatenate([shaped[:-1], shaped[1:]], axis=1)

    key_band = banded(extended_keys)
    value_band = banded(extended_values)
    query_block_list = queries.reshape(block_count, WINDOW_SPAN, kv_local, group_count, HEAD_SIZE)
    scores = jnp.einsum(
        "nqkgd,nskd->nkgqs", query_block_list, key_band, preferred_element_type=jnp.float32
    ) * HEAD_SIZE ** (-0.5)
    within = jnp.arange(WINDOW_SPAN)[:, None]
    column = jnp.arange(2 * WINDOW_SPAN)[None, :]
    distance = WINDOW_SPAN + within - column
    valid = (distance >= 0) & (distance < WINDOW_SPAN)
    key_pos = (
        offset
        + jnp.arange(block_count)[:, None] * WINDOW_SPAN
        + jnp.arange(2 * WINDOW_SPAN)[None, :]
        - WINDOW_SPAN
    )
    allowed = valid[None] & (key_pos >= 0)[:, None, :]
    allowed = allowed[:, None, None]
    head_sink_logit = sink_logit_table.reshape(kv_local, group_count)[None, :, :, None, None]
    masked = jnp.where(allowed, scores, -1e30)
    ceiling = jnp.maximum(jnp.max(masked, axis=-1, keepdims=True), head_sink_logit)
    powers = jnp.where(allowed, jnp.exp(masked - ceiling), 0.0)
    denom = jnp.sum(powers, axis=-1, keepdims=True) + jnp.exp(head_sink_logit - ceiling)
    probs = (powers / denom).astype(jnp.bfloat16)
    output = jnp.einsum("nkgqs,nskd->nqkgd", probs, value_band, preferred_element_type=jnp.float32)
    return output.astype(jnp.bfloat16).reshape(row_count, queries.shape[1])


def rounded(values):
    return lax.optimization_barrier(values.astype(jnp.bfloat16)).astype(jnp.float32)


def body(
    queries,
    key_heads,
    projected_value_heads,
    sink_logit_table,
    out_weight,
    residual,
    norm_gain,
    up_weight,
    down_weight,
):
    row_count = queries.shape[0]
    offset = lax.axis_index("sp") * row_count
    tail = jnp.concatenate(
        [key_heads[row_count - WINDOW_SPAN :], projected_value_heads[row_count - WINDOW_SPAN :]],
        axis=1,
    )
    previous = shifted(tail, "sp", 1)
    attended = attend(queries, key_heads, projected_value_heads, sink_logit_table, previous, offset)
    partial_value = rounded(jnp.dot(attended, out_weight, preferred_element_type=jnp.float32))
    mixed_sum = lax.psum_scatter(
        partial_value.astype(jnp.bfloat16), "tp", scatter_dimension=1, tiled=True
    ).astype(jnp.float32)
    stream = rounded(residual.astype(jnp.float32) + mixed_sum)
    squares = lax.psum(jnp.sum(stream * stream, axis=1, keepdims=True), "tp")
    normed = (stream * lax.rsqrt(squares / D + epsilon) * norm_gain.astype(jnp.float32)).astype(
        jnp.bfloat16
    )
    normed_whole = lax.all_gather(normed, "tp", axis=1, tiled=True)
    hidden_pre = jnp.dot(
        normed_whole,
        lax.all_gather(up_weight, "sp", axis=0, tiled=True),
        preferred_element_type=jnp.float32,
    )
    activated = jnp.square(jax.nn.relu(hidden_pre)).astype(jnp.bfloat16)
    terms = jnp.dot(
        activated,
        lax.all_gather(down_weight, "sp", axis=1, tiled=True),
        preferred_element_type=jnp.float32,
    )
    branch_sum = lax.psum_scatter(
        rounded(terms).astype(jnp.bfloat16), "tp", scatter_dimension=1, tiled=True
    ).astype(jnp.float32)
    return (stream + branch_sum).astype(jnp.bfloat16)


def solution(mesh):
    return jax.shard_map(
        body,
        mesh=mesh,
        in_specs=(
            P("sp", "tp"),
            P("sp", "tp"),
            P("sp", "tp"),
            P("tp"),
            P("tp", None),
            P("sp", "tp"),
            P("tp"),
            P("sp", "tp"),
            P("tp", "sp"),
        ),
        out_specs=P("sp", "tp"),
        check_vma=False,
    )
```

profile of v0, /device:TPU:0, one launch (start us, length us, event | category | flops | bytes accessed | tf_op | source)
XLA Modules:
  0.0 985.8 jit_solution(6724844009850247608)
XLA Ops:
  6.5 0.9 slice.32
  7.5 0.8 slice.33
  8.2 4.9 collective-permute-start
  13.3 1.0 broadcast_and_fusion
  14.3 2.0 reshape.91
  16.3 2.0 reshape.89
  18.3 1.4 copy.20
  19.7 1.1 copy.35
  20.8 1.9 copy.19
  22.7 0.7 max.26
  23.4 1.9 copy.15
  25.3 1.7 pad_maximum_fusion
  27.0 1.2 reshape.90
  28.2 1.0 copy.18
  29.2 2.5 fusion
  31.7 2.6 copy-done.3
  34.3 2.8 fusion.1
  37.9 4.9 fusion.8
  43.3 5.4 convolution_convert_fusion.1
  48.8 58.3 %reduce-scatter.3.cloned.1.call-done = bf16[1024,768]{1,0:T(8,128)(2,1)} async-done(((bf16[1024,3072]{1,0:T(8,128)(2,1)}), bf16[1024,768]{1,0:T(8,128)(2,1)}) %reduce-scatter.3.cloned.1.call-update) | async-done | bytes 1572880 | tf_op jit(solution)/shard_map/reduce_scatter | solution.py:83
  107.1 2.3 add_convert_fusion
  109.7 5.8 psum.7
  115.5 1.5 fusion.4
  117.1 0.7 all-gather.6.cloned.1.call-update
  117.9 0.5 all-gather.8.cloned.1.call-update
  118.6 45.6 %all-gather.4.cloned.1.call-done = bf16[1024,3072]{1,0:T(8,128)(2,1)} async-done(((bf16[1024,768]{1,0:T(8,128)(2,1)}), bf16[1024,3072]{1,0:T(8,128)(2,1)}) %all-gather.4.cloned.1.call-update) | async-done | bytes 6291472 | tf_op jit(solution)/shard_map/all_gather | solution.py:91
  164.2 364.0 %all-gather.6.cloned.1.call-done = bf16[3072,3072]{1,0:T(8,128)(2,1)} async-done(((bf16[384,3072]{1,0:T(8,128)(2,1)}), bf16[3072,3072]{1,0:T(8,128)(2,1)}) %all-gather.6.cloned.1.call-update) | async-done | bytes 18874384 | tf_op jit(solution)/shard_map/all_gather | solution.py:94
  528.2 25.8 %multiply_convert_fusion.clone.4 = bf16[1024,3072]{1,0:T(8,128)(2,1)} fusion(bf16[1024,3072]{1,0:T(8,128)(2,1)} %all-gather.4.cloned.1.call-done, bf16[3072,3072]{1,0:T(8,128)(2,1)} %all-gather.6.cloned.1.call-done), kind=kOutput, calls=%fused_computation.clone.clone.clone.1 | convolution fusion | flops 19336790016 | bytes 31457280 | tf_op jit(solution)/shard_map/dot_general | solution.py:92
  553.9 338.0 %all-gather.8.cloned.1.call-done = bf16[3072,3072]{1,0:T(8,128)(2,1)} async-done(((bf16[3072,384]{1,0:T(8,128)(2,1)}), bf16[3072,3072]{1,0:T(8,128)(2,1)}) %all-gather.8.cloned.1.call-update) | async-done | bytes 18874384 | tf_op jit(solution)/shard_map/all_gather | solution.py:100
  892.0 25.8 %convolution_convert_fusion = bf16[1024,3072]{1,0:T(8,128)(2,1)} fusion(bf16[3072,3072]{1,0:T(8,128)(2,1)} %all-gather.8.cloned.1.call-done, bf16[1024,3072]{1,0:T(8,128)(2,1)} %multiply_convert_fusion.clone.4), kind=kOutput, calls=%fused_computation.4 | convolution fusion | flops 19330498560 | bytes 31457280 | tf_op jit(solution)/shard_map/dot_general | solution.py:98
  917.9 58.0 %reduce-scatter.5.cloned.1.call-done = bf16[1024,768]{1,0:T(8,128)(2,1)} async-done(((bf16[1024,3072]{1,0:T(8,128)(2,1)}), bf16[1024,768]{1,0:T(8,128)(2,1)}) %reduce-scatter.5.cloned.1.call-update) | async-done | bytes 1572880 | tf_op jit(solution)/shard_map/reduce_scatter | solution.py:103
  975.9 3.4 fusion.5
  (36 shorter events, 2.2 us)
Async XLA Ops:
  6.5 36.7 %copy-start = (bf16[384,3072]{1,0:T(8,128)(2,1)S(1)}, bf16[384,3072]{1,0:T(8,128)(2,1)}, u32[]{:S(2)}) copy-start(bf16[384,3072]{1,0:T(8,128)(2,1)} %param.13) | copy-start | bytes 7077892
  6.5 18.8 %copy-start.4 = (bf16[1024,128]{1,0:T(8,128)(2,1)S(1)}, bf16[1024,128]{1,0:T(8,128)(2,1)}, u32[]{:S(2)}) copy-start(bf16[1024,128]{1,0:T(8,128)(2,1)} %param.10) | copy-start | bytes 786436
  6.5 100.5 %reduce-scatter.3.cloned.1.call-start = ((), (), s32[]{:S(2)}) async-start(), calls=%async_computation.2 | async-start | bytes 7864320 | tf_op jit(solution)/shard_map/reduce_scatter | solution.py:83
  8.2 17.1 %collective-permute-start = (bf16[128,256]{1,0:T(8,128)(2,1)S(1)}, bf16[128,256]{1,0:T(8,128)(2,1)S(1)}, u32[]{:S(2)}, u32[]{:S(2)}) collective-permute-start(bf16[128,256]{1,0:T(8,128)(2,1)S(1)} %pad_maximum_fusion.2), channel_id=1, source_target_pairs={{0,4},{4,8},{8,12},{12,16},{16,20},{20,24},{24,28},{1,5},{5,9},{9,... | collective-permute-start | bytes 196616 | tf_op jit(solution)/shard_map/ppermute | solution.py:15
  29.1 8.7 copy-start.5
  31.6 2.7 copy-start.3
  43.3 5.5 copy-start.6
  48.7 115.5 %all-gather.4.cloned.1.call-start = ((), (), s32[]{:S(2)}) async-start(), calls=%async_computation.3 | async-start | bytes 7864320 | tf_op jit(solution)/shard_map/all_gather | solution.py:91
  109.3 444.6 %copy-start.2 = (bf16[1024,768]{1,0:T(8,128)(2,1)}, bf16[1024,768]{1,0:T(8,128)(2,1)S(1)}, u32[]{:S(2)}) copy-start(bf16[1024,768]{1,0:T(8,128)(2,1)S(1)} %add_convert_fusion) | copy-start | bytes 4718596
  117.1 411.1 %all-gather.6.cloned.1.call-start = ((), (), s32[]{:S(2)}) async-start(), calls=%async_computation.4 | async-start | bytes 21233664 | tf_op jit(solution)/shard_map/all_gather | solution.py:94
  117.8 774.2 %all-gather.8.cloned.1.call-start = ((), (), s32[]{:S(2)}) async-start(), calls=%async_computation.5 | async-start | bytes 21233664 | tf_op jit(solution)/shard_map/all_gather | solution.py:100
  118.4 857.5 %reduce-scatter.5.cloned.1.call-start = ((), (), s32[]{:S(2)}) async-start(), calls=%async_computation.6 | async-start | bytes 7864320 | tf_op jit(solution)/shard_map/reduce_scatter | solution.py:103
  892.0 87.3 %copy-start.1 = (bf16[384,3072]{1,0:T(8,128)(2,1)S(1)}, bf16[384,3072]{1,0:T(8,128)(2,1)}, u32[]{:S(2)}) copy-start(bf16[384,3072]{1,0:T(8,128)(2,1)} %param.13) | copy-start | bytes 7077892
Sparse Core Ops, SparseCore 0:
  48.8 58.1 reduce-scatter.2
  117.2 46.9 all-gather.3
  165.8 362.3 all-gather.5
  529.6 362.3 all-gather.7
  918.0 57.8 reduce-scatter.4
where the time goes:
time: 986 us
  waiting for transfers between devices  865 us (88%)
  matrix products  64.4 us (7%)
  local copies, waits for them, and re-layouts  18.5 us (2%)
  other arithmetic  13.4 us (1%)
  between operations  13.3 us (1%)
    all_gather x1, waiting for transfers between devices, body(): lax.all_gather(up_weight, 'sp', axis=0, tiled=True)  364 us
    all_gather x1, waiting for transfers between devices, body(): lax.all_gather(down_weight, 'sp', axis=1, tiled=True)  338 us
    reduce_scatter x1, waiting for transfers between devices, body(): lax.psum_scatter(partial_value.astype(jnp.bfloat16), 'tp', scatter_dimens...  58.3 us
    reduce_scatter x1, waiting for transfers between devices, body(): lax.psum_scatter(rounded(terms).astype(jnp.bfloat16), 'tp', scatter_dimen...  58 us
    all_gather x1, waiting for transfers between devices, body(): normed_whole = lax.all_gather(normed, 'tp', axis=1, tiled=True)  45.6 us
    dot_general x1, matrix products, body(): jnp.dot(activated, lax.all_gather(down_weight, 'sp', axis=1, tiled=True),...  25.8 us
    dot_general x1, matrix products, body(): jnp.dot(normed_whole, lax.all_gather(up_weight, 'sp', axis=0, tiled=True)...  25.8 us
  transfers between devices with their start and end apart: 6, of which 5 were waited for; matrix products, arithmetic and copies ran while one was open for 4% of the time, Pallas kernels for 0%

commit v1 on v0

--- a/solution.py
+++ b/solution.py
@@ -97,7 +97,9 @@
     activated = jnp.square(jax.nn.relu(hidden_pre)).astype(jnp.bfloat16)
     terms = jnp.dot(
         activated,
-        lax.all_gather(down_weight, "sp", axis=1, tiled=True),
+        jnp.concatenate(
+            lax.all_to_all(jnp.stack([down_weight] * lax.axis_size("sp")), "sp", 0, 0), axis=1
+        ),
         preferred_element_type=jnp.float32,
     )
     branch_sum = lax.psum_scatter(

time: 986 us -> 877 us (0.89)
  waiting for transfers between devices: 865 us -> 748 us
    all_gather x1 -> x0, waiting for transfers between devices: 338 us -> none  [body(): lax.all_gather(down_weight, 'sp', axis=1, tiled=True)]
    all_gather x1, waiting for transfers between devices: 364 us -> 590 us  [body(): lax.all_gather(up_weight, 'sp', axis=0, tiled=True)]
    all_gather x1, waiting for transfers between devices: 45.6 us -> 26.9 us  [body(): normed_whole = lax.all_gather(normed, 'tp', axis=1, tiled=True)]
    reduce_scatter x1, waiting for transfers between devices: 58 us -> 71.6 us  [body(): lax.psum_scatter(rounded(terms).astype(jnp.bfloat16), 'tp', scatter_dimen...]
  transfers between devices with their start and end apart: 6 -> 6, of which waited for: 5 -> 4; matrix products, arithmetic and copies ran while one was open for 4% -> 5% of each run, Pallas kernels for 0% -> 0%
where the time goes in v1:
time: 877 us
  waiting for transfers between devices  748 us (85%)
  matrix products  61.6 us (7%)
  local copies, waits for them, and re-layouts  24.9 us (3%)
  between operations  13.3 us (2%)
  other arithmetic  11.9 us (1%)
  starting transfers between devices  11.1 us (1%)
    all_gather x1, waiting for transfers between devices, body(): lax.all_gather(up_weight, 'sp', axis=0, tiled=True)  590 us
    reduce_scatter x1, waiting for transfers between devices, body(): lax.psum_scatter(rounded(terms).astype(jnp.bfloat16), 'tp', scatter_dimen...  71.6 us
    reduce_scatter x1, waiting for transfers between devices, body(): lax.psum_scatter(partial_value.astype(jnp.bfloat16), 'tp', scatter_dimens...  58.3 us
    all_gather x1, waiting for transfers between devices, body(): normed_whole = lax.all_gather(normed, 'tp', axis=1, tiled=True)  26.9 us
    dot_general x1, matrix products, body(): jnp.dot(activated, jnp.concatenate(lax.all_to_all(jnp.stack([down_weight]...  25.9 us
    dot_general x1, matrix products, body(): jnp.dot(normed_whole, lax.all_gather(up_weight, 'sp', axis=0, tiled=True)...  25.7 us
  transfers between devices with their start and end apart: 6, of which 4 were waited for; matrix products, arithmetic and copies ran while one was open for 5% of the time, Pallas kernels for 0%

profile of v1, /device:TPU:0, one launch (start us, length us, event | category | flops | bytes accessed | tf_op | source)
XLA Modules:
  0.0 876.6 jit_solution(13488720457461711960)
XLA Ops:
  6.5 0.9 slice.32
  7.5 0.8 slice.33
  8.2 4.9 collective-permute-start
  13.3 1.0 broadcast_and_fusion
  14.3 1.2 reshape.101
  15.5 1.2 reshape.99
  16.7 0.7 max.26
  17.4 1.0 copy.19
  18.4 1.0 copy.15
  19.4 1.4 copy.20
  20.8 1.1 copy.36
  21.9 1.1 pad_maximum_fusion
  23.2 1.0 copy.18
  24.8 2.5 fusion
  27.4 1.8 fusion.1
  29.3 2.2 fusion.8
  31.5 0.5 copy.23
  32.1 5.4 convolution_convert_fusion.1
  37.5 58.3 %reduce-scatter.3.cloned.1.call-done = bf16[1024,768]{1,0:T(8,128)(2,1)} async-done(((bf16[1024,3072]{1,0:T(8,128)(2,1)}), bf16[1024,768]{1,0:T(8,128)(2,1)}) %reduce-scatter.3.cloned.1.call-update) | async-done | bytes 1572880 | tf_op jit(solution)/shard_map/reduce_scatter | solution.py:83
  95.8 2.3 add_convert_fusion
  98.5 5.8 psum.7
  104.3 1.6 fusion.4
  105.9 0.7 all-gather.5.cloned.1.call-update
  106.6 4.3 copy.24
  110.9 9.1 %stack.2 = bf16[8,3072,384]{1,2,0:T(8,128)(2,1)} broadcast(bf16[3072,384]{0,1:T(8,128)(2,1)} %copy.24), dimensions={1,2} | broadcast | bytes 21233664 | tf_op jit(solution)/shard_map/stack | solution.py:101
  120.0 5.9 all-to-all-start
  126.1 26.9 %all-gather.3.cloned.1.call-done = bf16[1024,3072]{1,0:T(8,128)(2,1)} async-done(((bf16[1024,768]{1,0:T(8,128)(2,1)}), bf16[1024,3072]{1,0:T(8,128)(2,1)}) %all-gather.3.cloned.1.call-update) | async-done | bytes 6291472 | tf_op jit(solution)/shard_map/all_gather | solution.py:91
  153.0 590.5 %all-gather.5.cloned.1.call-done = bf16[3072,3072]{1,0:T(8,128)(2,1)} async-done(((bf16[384,3072]{1,0:T(8,128)(2,1)}), bf16[3072,3072]{1,0:T(8,128)(2,1)}) %all-gather.5.cloned.1.call-update) | async-done | bytes 18874384 | tf_op jit(solution)/shard_map/all_gather | solution.py:94
  743.5 25.7 %multiply_convert_fusion.clone.4 = bf16[1024,3072]{1,0:T(8,128)(2,1)} fusion(bf16[1024,3072]{1,0:T(8,128)(2,1)} %all-gather.3.cloned.1.call-done, bf16[3072,3072]{1,0:T(8,128)(2,1)} %all-gather.5.cloned.1.call-done), kind=kOutput, calls=%fused_computation.clone.clone.clone.1 | convolution fusion | flops 19336790016 | bytes 31457280 | tf_op jit(solution)/shard_map/dot_general | solution.py:92
  769.2 25.9 %convolution_convert_fusion = bf16[1024,3072]{1,0:T(8,128)(2,1)} fusion(bf16[3072,3072]{0,1:T(8,128)(2,1)} %bitcast.9, bf16[1024,3072]{1,0:T(8,128)(2,1)} %multiply_convert_fusion.clone.4), kind=kOutput, calls=%fused_computation.4 | convolution fusion | flops 19330498560 | bytes 31457280 | tf_op jit(solution)/shard_map/dot_general | solution.py:98
  795.1 71.6 %reduce-scatter.5.cloned.1.call-done = bf16[1024,768]{1,0:T(8,128)(2,1)} async-done(((bf16[1024,3072]{1,0:T(8,128)(2,1)}), bf16[1024,768]{1,0:T(8,128)(2,1)}) %reduce-scatter.5.cloned.1.call-update) | async-done | bytes 1572880 | tf_op jit(solution)/shard_map/reduce_scatter | solution.py:105
  866.7 3.4 fusion.5
  (35 shorter events, 1.9 us)
Async XLA Ops:
  6.5 25.5 %copy-start = (bf16[384,3072]{1,0:T(8,128)(2,1)S(1)}, bf16[384,3072]{1,0:T(8,128)(2,1)}, u32[]{:S(2)}) copy-start(bf16[384,3072]{1,0:T(8,128)(2,1)} %param.13) | copy-start | bytes 7077892
  6.5 89.3 %reduce-scatter.3.cloned.1.call-start = ((), (), s32[]{:S(2)}) async-start(), calls=%async_computation.3 | async-start | bytes 7864320 | tf_op jit(solution)/shard_map/reduce_scatter | solution.py:83
  8.2 13.6 %collective-permute-start = (bf16[128,256]{1,0:T(8,128)(2,1)S(1)}, bf16[128,256]{1,0:T(8,128)(2,1)S(1)}, u32[]{:S(2)}, u32[]{:S(2)}) collective-permute-start(bf16[128,256]{1,0:T(8,128)(2,1)S(1)} %pad_maximum_fusion.2), channel_id=1, source_target_pairs={{0,4},{4,8},{8,12},{12,16},{16,20},{20,24},{24,28},{1,5},{5,9},{9,... | collective-permute-start | bytes 196616 | tf_op jit(solution)/shard_map/ppermute | solution.py:15
  23.2 4.2 copy-start.3
  24.8 4.5 copy-start.4
  32.0 5.5 copy-start.5
  37.5 115.6 %all-gather.3.cloned.1.call-start = ((), (), s32[]{:S(2)}) async-start(), calls=%async_computation.4 | async-start | bytes 7864320 | tf_op jit(solution)/shard_map/all_gather | solution.py:91
  98.1 12.8 %copy-start.2 = (bf16[1024,768]{1,0:T(8,128)(2,1)}, bf16[1024,768]{1,0:T(8,128)(2,1)S(1)}, u32[]{:S(2)}) copy-start(bf16[1024,768]{1,0:T(8,128)(2,1)S(1)} %add_convert_fusion) | copy-start | bytes 4718596
  105.9 637.6 %all-gather.5.cloned.1.call-start = ((), (), s32[]{:S(2)}) async-start(), calls=%async_computation.5 | async-start | bytes 21233664 | tf_op jit(solution)/shard_map/all_gather | solution.py:94
  120.0 649.2 %all-to-all-start = ((bf16[8,3072,384]{1,2,0:T(8,128)(2,1)}), bf16[8,3072,384]{1,2,0:T(8,128)(2,1)}, u32[]{:S(2)}, u32[]{:S(2)}) async-start(bf16[8,3072,384]{1,2,0:T(8,128)(2,1)} %stack.2), calls=%async_computation.1 | async-start | bytes 37748736 | tf_op jit(solution)/shard_map/all_to_all | solution.py:101
  125.9 740.8 %reduce-scatter.5.cloned.1.call-start = ((), (), s32[]{:S(2)}) async-start(), calls=%async_computation.6 | async-start | bytes 7864320 | tf_op jit(solution)/shard_map/reduce_scatter | solution.py:105
  769.2 100.9 %copy-start.1 = (bf16[384,3072]{1,0:T(8,128)(2,1)S(1)}, bf16[384,3072]{1,0:T(8,128)(2,1)}, u32[]{:S(2)}) copy-start(bf16[384,3072]{1,0:T(8,128)(2,1)} %param.13) | copy-start | bytes 7077892
Sparse Core Ops, SparseCore 0:
  37.6 58.1 reduce-scatter.2
  106.0 46.9 all-gather.2
  154.6 588.8 all-gather.4
  795.2 71.4 reduce-scatter.4
